TPU v7x, 256 devices: a whole 4x4x8 slice. The times are simulated.
256 devices in a mesh: sp: 32 (over z, x), tp: 8 (over y, core).
Axes of the slice: x: 4, y: 4, z: 8, core: 2. Of those that a mesh axis runs over, the one named last changes fastest.
Arguments:
- tokens: bfloat16 [8192, 4096], P('sp', 'tp'), may hold values from -6 to 6
- pre_gain: float32 [4096], replicated, may hold values from 0.1 to 1.9
- rate_factor: float32 [8192], P('sp'), may hold values from 0.5 to 2, as said below
- w_rec_in: bfloat16 [4096, 1024], P(None, 'tp'), may hold values from -0.09375 to 0.09375
- w_rec_gate: bfloat16 [4096, 1024], P(None, 'tp')
- conv_taps: float32 [4, 1024], P(None, 'tp'), may hold values from -3 to 3
- rate_maps: bfloat16 [8, 128, 128], P('tp'), may hold values from -0.5 to 0.5
- input_maps: bfloat16 [8, 128, 128], P('tp'), may hold values from -0.5 to 0.5
- decay_param: float32 [1024], P('tp'), as said below
- w_query: bfloat16 [4096, 1536], P(None, 'tp'), may hold values from -0.09375 to 0.09375
- w_latent: bfloat16 [4096, 512], replicated, may hold values from -0.09375 to 0.09375
- w_rope_key: bfloat16 [4096, 64], replicated, may hold values from -0.09375 to 0.09375
- latent_gain: float32 [512], replicated, may hold values from 0.7 to 100, as said below
- w_expand: bfloat16 [512, 2048], P(None, 'tp')
- rec_gain: float32 [1024], P('tp'), may hold values from 0.1 to 1.9
- att_gain: float32 [1024], P('tp'), may hold values from 0.1 to 1.9
- w_out_rec: bfloat16 [1024, 4096], P('tp'), may hold values from -0.125 to 0.125
- w_out_att: bfloat16 [1024, 4096], P('tp'), may hold values from -0.125 to 0.125
- post_gain: float32 [4096], replicated, may hold values from 0.1 to 1.9
Outputs:
- layer_out: bfloat16 [8192, 4096], P(('sp', 'tp'))
Inputs may be any that keep to these rules, and one draw needn't show every extreme that they name: `rate_factor`: one positive factor for each position. `decay_param`: one parameter for each recurrent channel. `latent_gain`: one positive gain for each latent entry.
All inputs are finite; a program needn't handle non-finite values.
Results may differ from a plain program's by a relative error of at most 0.017.
The roundings to bfloat16 on the way count: a program that leaves them out, or rounds other values in their place, can miss the bound.
Values may be sent and summed in bfloat16 or wider, within the bound.
A program may use at most 128 MiB of HBM per device.

v0:
```python
import math
import jax
import jax.numpy as jnp
from jax import lax
from jax.sharding import PartitionSpec as P

NOPE = 128
ROPE = 64
VDIM = 128
EPS = 1e-06
RATE_C = 8.0
THETA = 10000.0
span_limit = 2048


def passed_along(block, axis, distance):
    devices = range(lax.axis_size(axis))
    route = [(i - distance, i) for i in devices if i - distance in devices]
    return lax.ppermute(block, axis, route)


def from_everyone(shard, axis):
    copies = jnp.broadcast_to(shard, (lax.axis_size(axis), *shard.shape))
    return lax.all_to_all(copies, axis, split_axis=0, concat_axis=0, tiled=True)


def all_in_one(shard, axis):
    leaves = jax.tree.leaves(shard)
    order = sorted(range(len(leaves)), key=lambda k: -leaves[k].size)
    width = (1, *leaves[order[0]].shape)[-1]
    lines = [
        jnp.pad(leaves[k].reshape(-1), (0, -leaves[k].size % width)).reshape(-1, width)
        for k in order
    ]
    both, at, found = (from_everyone(jnp.concatenate(lines), axis), 0, {})
    for k, line in zip(order, lines):
        slab = both[:, at : at + len(line)].reshape(len(both), -1)
        found[k] = slab[:, : leaves[k].size].reshape(-1, *leaves[k].shape)
        at += len(line)
    numbers = iter(range(len(leaves)))
    return jax.tree.map(lambda _: found[next(numbers)], shard)


def joined_by_halves(pieces, combine):
    while len(jax.tree.leaves(pieces)[0]) > 1:
        pieces = jax.vmap(combine)(
            *(jax.tree.map(lambda part: part[side::2], pieces) for side in (0, 1))
        )
    return jax.tree.map(lambda part: part[0], pieces)


def entering(shard, axis, combine, identity):
    count, mine = (lax.axis_size(axis), lax.axis_index(axis))
    passed = jnp.arange(count) < mine

    def kept(part, zero, own):
        part = jnp.where(
            passed.reshape(-1, *(1 for _ in own.shape)), part, jnp.asarray(zero, own.dtype)
        )
        return part

    pieces = all_in_one(shard, axis)
    return joined_by_halves(jax.tree.map(kept, pieces, identity, shard), combine)


def of_everyone(shard, axis):
    return from_everyone(shard, axis).sum(axis=0)


def in_one_piece(arrays, axis, dim, along):
    widths = [a.shape[along] for a in arrays]
    both = jnp.concatenate(arrays, axis=along)
    out = lax.all_gather(both, axis, axis=dim, tiled=True)
    return tuple(jnp.split(out, [sum(widths[:k]) for k in range(1, len(widths))], axis=along))


def in_blocks(shard, dim, count):
    before, after = (shard.shape[:dim], shard.shape[dim + 1 :])
    return jnp.moveaxis(shard.reshape(*before, count, -1, *after), dim, 0)


def sum_at_owner(shard, axis, dim):
    count = lax.axis_size(axis)
    pieces = lax.all_to_all(in_blocks(shard, dim, count), axis, 0, 0, tiled=True)
    return jnp.sum(pieces.astype(jnp.float32), axis=0)


def rms_inverse(values):
    return lax.rsqrt(jnp.mean(values * values, axis=-1, keepdims=True) + EPS)


def rotate(values, cosine, sine_part):
    half_width = values.shape[-1] // 2
    leading = values[..., :half_width]
    trailing = values[..., half_width:]
    return jnp.concatenate(
        [leading * cosine - trailing * sine_part, trailing * cosine + leading * sine_part], axis=-1
    )


def angles(length, offset, span_width):
    frequency = 1.0 / THETA ** (jnp.arange(0, span_width, 2).astype(jnp.float32) / span_width)
    places = (offset + jnp.arange(length)).astype(jnp.float32)
    turned = places[:, None] * frequency[None, :]
    return (jnp.cos(turned), jnp.sin(turned))


def combine_steps(earlier, later):
    return (earlier[0] * later[0], later[0] * earlier[1] + later[1])


def attend_block(state_now, query_nope, query_rope, places, keys_nope, key_rope, values, key_root):
    maxima, totals, accumulated = state_now
    scaling = 1.0 / math.sqrt(query_nope.shape[-1] + query_rope.shape[-1])
    scores = jnp.einsum("qhd,khd->hqk", query_nope, keys_nope, preferred_element_type=jnp.float32)
    scores = scores + jnp.einsum(
        "qhd,kd->hqk", query_rope, key_rope, preferred_element_type=jnp.float32
    )
    scores = scores * scaling
    key_places = key_root + jnp.arange(keys_nope.shape[0])
    visible = key_places[None, :] <= places[:, None]
    scores = jnp.where(visible[None], scores, -jnp.inf)
    largest = jnp.maximum(maxima, jnp.max(scores, axis=-1))
    anchor = jnp.where(largest == -jnp.inf, 0.0, largest)
    weights = jnp.exp(scores - anchor[..., None])
    shrink = jnp.exp(maxima - anchor)
    totals = totals * shrink + jnp.sum(weights, axis=-1)
    accumulated = accumulated * shrink[..., None] + jnp.einsum(
        "hqk,khd->hqd", weights.astype(jnp.bfloat16), values, preferred_element_type=jnp.float32
    )
    return (largest, totals, accumulated)


def shards(
    tokens,
    pre_gain,
    rate_factor,
    w_rec_in,
    w_rec_gate,
    conv_taps,
    rate_maps,
    input_maps,
    decay_param,
    w_query,
    w_latent,
    w_rope_key,
    latent_gain,
    w_expand,
    rec_gain,
    att_gain,
    w_out_rec,
    w_out_att,
    post_gain,
):
    row_count = tokens.shape[0]
    model_width = w_rec_in.shape[0]
    channels = w_rec_in.shape[1]
    heads_here = w_query.shape[1] // (NOPE + ROPE)
    group_size = lax.axis_size("tp")
    first_place = lax.axis_index("sp") * row_count
    places = first_place + jnp.arange(row_count)
    last_place = first_place + row_count - 1
    piece_wide = lax.all_gather(tokens, "tp", axis=1, tiled=True).astype(jnp.float32)
    piece_low = (piece_wide * pre_gain).astype(jnp.bfloat16)

    def accumulate(source, weight):
        return jnp.dot(source, weight, preferred_element_type=jnp.float32)

    squares = jnp.sum(piece_wide * piece_wide, axis=1, keepdims=True)
    sum_input = accumulate(piece_low, w_rec_in)
    sum_gate = accumulate(piece_low, w_rec_gate)
    sum_query = accumulate(piece_low, w_query)
    sum_latent = accumulate(piece_low, w_latent)
    sum_rope = accumulate(piece_low, w_rope_key)
    inverse = lax.rsqrt(squares / model_width + EPS)
    rec_input = (inverse * sum_input).astype(jnp.bfloat16)
    gate_value = inverse * sum_gate
    query_raw = inverse * sum_query
    latent_raw = inverse * sum_latent
    rope_raw = inverse * sum_rope
    taps = conv_taps.shape[0]
    tail_rows = rec_input[row_count - (taps - 1) :]
    before = passed_along(tail_rows, "sp", 1)
    padded = jnp.concatenate([before, rec_input], axis=0)
    convolved = conv_taps[0] * padded[0:row_count].astype(jnp.float32)
    for tap_index in range(1, taps):
        convolved = convolved + conv_taps[tap_index] * padded[
            tap_index : tap_index + row_count
        ].astype(jnp.float32)
    conv_low = convolved.astype(jnp.bfloat16)
    blocks = conv_low.reshape(row_count, rate_maps.shape[0], rate_maps.shape[1])
    rate_gate = jax.nn.sigmoid(
        jnp.einsum("sbi,bij->sbj", blocks, rate_maps, preferred_element_type=jnp.float32)
    ).reshape(row_count, channels)
    entry_gate = jax.nn.sigmoid(
        jnp.einsum("sbi,bij->sbj", blocks, input_maps, preferred_element_type=jnp.float32)
    ).reshape(row_count, channels)
    log_keep = -RATE_C * rate_factor[:, None] * rate_gate * jax.nn.softplus(-decay_param)
    keep_rate = jnp.exp(log_keep)
    driven = jnp.sqrt(-jnp.expm1(2.0 * log_keep)) * entry_gate * convolved
    cum_keep, local_state = lax.associative_scan(combine_steps, (keep_rate, driven), axis=0)
    identity = (jnp.ones((channels,), jnp.float32), jnp.zeros((channels,), jnp.float32))
    chain_keep, carried = entering(
        (cum_keep[row_count - 1], local_state[row_count - 1]), "sp", combine_steps, identity
    )
    state_seq = local_state + cum_keep * carried[None, :]
    rec_out = state_seq * jax.nn.gelu(gate_value)
    rec_squares = jnp.sum(rec_out * rec_out, axis=1, keepdims=True)
    rec_total = of_everyone(rec_squares, "tp")
    cosine, sine_part = angles(row_count, first_place, ROPE)
    query_heads = query_raw.reshape(row_count, heads_here, NOPE + ROPE)
    query_nope = query_heads[:, :, :NOPE].astype(jnp.bfloat16)
    query_rope = rotate(query_heads[:, :, NOPE:], cosine[:, None, :], sine_part[:, None, :]).astype(
        jnp.bfloat16
    )
    own_latent = (latent_raw * rms_inverse(latent_raw) * latent_gain).astype(jnp.bfloat16)
    rope_key = rotate(rope_raw, cosine, sine_part).astype(jnp.bfloat16)
    start_state = (
        jnp.full((heads_here, row_count), -jnp.inf, jnp.float32),
        jnp.zeros((heads_here, row_count), jnp.float32),
        jnp.zeros((heads_here, row_count, VDIM), jnp.float32),
    )
    expanded_local = jnp.dot(own_latent, w_expand, preferred_element_type=jnp.float32).astype(
        jnp.bfloat16
    )
    key_source, rope_source = in_one_piece((expanded_local, rope_key), "sp", 0, 1)
    total_rows = key_source.shape[0]
    key_span = math.gcd(total_rows, span_limit)

    def one_span(span_index, state_inner):
        key_root = span_index * key_span

        def compute(state_deep):
            source_rows = lax.dynamic_slice_in_dim(key_source, span_index * key_span, key_span, 0)
            rope_rows = lax.dynamic_slice_in_dim(rope_source, span_index * key_span, key_span, 0)
            expanded = source_rows
            expanded = expanded.reshape(key_span, heads_here, NOPE + VDIM)
            return attend_block(
                state_deep,
                query_nope,
                query_rope,
                places,
                expanded[:, :, :NOPE],
                rope_rows,
                expanded[:, :, NOPE:],
                key_root,
            )

        def keep_state(state_deep):
            return state_deep

        return lax.cond(key_root <= last_place, compute, keep_state, state_inner)

    maxima, totals, accumulated = lax.fori_loop(0, total_rows // key_span, one_span, start_state)
    att_out = (
        (accumulated / totals[..., None]).transpose(1, 0, 2).reshape(row_count, heads_here * VDIM)
    )
    att_squares = jnp.sum(att_out * att_out, axis=1, keepdims=True)
    att_total = of_everyone(att_squares, "tp")
    rec_norm = (rec_out * lax.rsqrt(rec_total / (channels * group_size) + EPS) * rec_gain).astype(
        jnp.bfloat16
    )
    att_norm = (
        att_out * lax.rsqrt(att_total / (heads_here * VDIM * group_size) + EPS) * att_gain
    ).astype(jnp.bfloat16)
    mixed_sum = sum_at_owner(
        (
            jnp.dot(rec_norm, w_out_rec, preferred_element_type=jnp.float32)
            + jnp.dot(att_norm, w_out_att, preferred_element_type=jnp.float32)
        ).astype(jnp.bfloat16),
        "tp",
        0,
    )
    return (mixed_sum * rms_inverse(mixed_sum) * post_gain).astype(jnp.bfloat16)


def solution(mesh):
    placed = (
        P("sp", "tp"),
        P(),
        P("sp"),
        P(None, "tp"),
        P(None, "tp"),
        P(None, "tp"),
        P("tp", None, None),
        P("tp", None, None),
        P("tp"),
        P(None, "tp"),
        P(),
        P(),
        P(),
        P(None, "tp"),
        P("tp"),
        P("tp"),
        P("tp", None),
        P("tp", None),
        P(),
    )
    return jax.shard_map(
        shards, mesh=mesh, in_specs=placed, out_specs=P(("sp", "tp"), None), check_vma=False
    )
```

profile of v0, /device:TPU:228, one launch (start us, length us, event | category | flops | bytes accessed | tf_op | source)
XLA Modules:
  0.0 218.6 jit_solution(17442014184566971345)
XLA Ops:
  7.3 30.1 %all-gather.3.cloned.1.call-done = bf16[256,4096]{1,0:T(8,128)(2,1)} async-done(((bf16[256,512]{1,0:T(8,128)(2,1)}), bf16[256,4096]{1,0:T(8,128)(2,1)}) %all-gather.3.cloned.1.call-update) | async-done | bytes 2097168 | tf_op jit(solution)/shard_map/all_gather | solution.py:163
  37.5 2.2 %fusion.16 = f32[256]{0:T(256)S(1)} fusion(bf16[256,4096]{1,0:T(8,128)(2,1)} %all-gather.3.cloned.1.call-done), kind=kLoop, calls=%fused_computation.29 | loop fusion | flops 3145472 | bytes 2098176 | tf_op jit(solution)/shard_map/reduce_sum | solution.py:169
  39.7 3.6 %multiply_reduce_fusion.1 = (f32[256]{0:T(256)S(1)}, f32[256,512]{1,0:T(8,128)S(1)}) fusion(bf16[4096,512]{1,0:T(8,128)(2,1)} %param.33, bf16[256,4096]{1,0:T(8,128)(2,1)S(1)} %copy-done.1, f32[4096]{0:T(1024)S(1)} %copy-done.14, f32[256]{0:T(256)S(1)} %add_rsqrt_fusion.3), kind=kOutput, calls=%fused_computation.55 | convolution fusion | flops 1077280512 | bytes 6834176 | tf_op jit(solution)/shard_map/dot_general | solution.py:167
  45.6 2.7 %fusion.29 = bf16[256,128]{1,0:T(8,128)(2,1)S(1)} fusion(bf16[4096,128]{1,0:T(8,128)(2,1)} %param.26, bf16[256,4096]{1,0:T(8,128)(2,1)} %all-gather.3.cloned.1.call-done, f32[4096]{0:T(1024)S(1)} %copy-done.14, f32[256]{0:T(256)S(1)} %add_rsqrt_fusion.3), kind=kOutput, calls=%fused_computation.50 | convolution fusion | flops 271646720 | bytes 3228672 | tf_op jit(solution)/shard_map/dot_general | solution.py:167
  48.3 3.1 %collective-permute-start = (bf16[3,128]{1,0:T(4,128)(2,1)S(1)}, bf16[3,128]{1,0:T(4,128)(2,1)S(1)}, u32[]{:S(2)}, u32[]{:S(2)}) collective-permute-start(bf16[3,128]{1,0:T(4,128)(2,1)S(1)} %slice.463), channel_id=1, source_target_pairs={{0,8},{8,16},{16,24},{24,32},{32,40},{40,48},{48,56},{56,64},{64,7... | collective-permute-start | bytes 2312 | tf_op jit(solution)/shard_map/ppermute | solution.py:19
  56.8 10.5 %all-to-all-start = ((f32[32,2,128]{2,1,0:T(2,128)}), f32[32,2,128]{2,1,0:T(2,128)S(1)}, u32[]{:S(2)}, u32[]{:S(2)}) async-start(f32[32,2,128]{2,1,0:T(2,128)} %broadcast_in_dim.42), calls=%async_computation | async-start | bytes 65536 | tf_op jit(solution)/shard_map/all_to_all | solution.py:24
  67.5 5.4 %all-to-all-done = f32[32,2,128]{2,1,0:T(2,128)S(1)} async-done(((f32[32,2,128]{2,1,0:T(2,128)}), f32[32,2,128]{2,1,0:T(2,128)S(1)}, u32[]{:S(2)}, u32[]{:S(2)}) %all-to-all-start) | async-done | bytes 32800 | tf_op jit(solution)/shard_map/all_to_all | solution.py:24
  73.3 2.7 %multiply_reduce_fusion.2 = (f32[256]{0:T(256)S(1)}, f32[256,128]{1,0:T(8,128)S(1)}) fusion(bf16[4096,128]{1,0:T(8,128)(2,1)} %param.27, bf16[256,4096]{1,0:T(8,128)(2,1)} %all-gather.3.cloned.1.call-done, f32[4096]{0:T(1024)S(1)} %copy-done.14, f32[256]{0:T(256)S(1)} %add_rsqrt_fusion.3, f32[128]{0:T(128)S(1)} %add_bitcast_fusion, ...), kind=kOutput, calls=%fused_computation.75 | convolution fusion | flops 272105216 | bytes 3820032 | tf_op jit(solution)/shard_map/dot_general | solution.py:167
  76.6 3.4 %all-to-all-start.1 = ((f32[8,256,1]{1,2,0:T(1,128)}), f32[8,256,1]{1,2,0:T(1,128)S(1)}, u32[]{:S(2)}, u32[]{:S(2)}) async-start(f32[8,256,1]{1,2,0:T(1,128)} %broadcast_in_dim.45), calls=%async_computation.1 | async-start | bytes 16384 | tf_op jit(solution)/shard_map/all_to_all | solution.py:24
  80.2 5.2 %all-to-all-done.1 = f32[8,256,1]{1,2,0:T(1,128)S(1)} async-done(((f32[8,256,1]{1,2,0:T(1,128)}), f32[8,256,1]{1,2,0:T(1,128)S(1)}, u32[]{:S(2)}, u32[]{:S(2)}) %all-to-all-start.1) | async-done | bytes 8224 | tf_op jit(solution)/shard_map/all_to_all | solution.py:24
  85.4 49.2 %all-gather.5.cloned.1.call-done = bf16[8192,320]{0,1:T(8,128)(2,1)} async-done(((bf16[256,320]{0,1:T(8,128)(2,1)}), bf16[8192,320]{0,1:T(8,128)(2,1)}) %all-gather.5.cloned.1.call-update) | async-done | bytes 5242896 | tf_op jit(solution)/shard_map/all_gather | solution.py:73
  134.6 4.7 %split.8 = bf16[8192,256]{0,1:T(8,128)(2,1)} slice(bf16[8192,320]{0,1:T(8,128)(2,1)} %all-gather.5.cloned.1.call-done), slice={[0:8192], [0:256]} | slice | bytes 8388608 | tf_op jit(solution)/shard_map/split | solution.py:74
  139.3 6.4 %copy.31 = bf16[8192,256]{1,0:T(8,128)(2,1)} copy(bf16[8192,256]{0,1:T(8,128)(2,1)} %split.8) | data formatting | bytes 8388608
  146.9 1.8 copy.33
  148.7 17.6 %while.18 = (s32[]{:T(128)}, f32[1,256]{1,0:T(1,128)S(1)}, f32[1,256]{1,0:T(1,128)S(1)}, f32[1,256,128]{2,1,0:T(8,128)S(1)}, s32[]{:T(128)}, /*index=5*/bf16[819...) while((s32[]{:T(128)}, f32[1,256]{1,0:T(1,128)S(1)}, ...), condition=%wide.region_9.10_spmd.clone, body=%wide.region_4.9_spmd.clone.sunk | while | flops 340332288 | bytes 14554469 | solution.py:254
  148.7 4.4 %conditional.3 = ((f32[1,256]{1,0:T(1,128)S(1)}, f32[1,256]{1,0:T(1,128)S(1)}, f32[1,256,128]{2,1,0:T(8,128)S(1)})) conditional(s32[]{:T(128)} %convert_element_type.205, (f32[1,256]{1,0:T(1,128)S(1)}, f32[1,256]{1,0:T(1,128)S(1)}, f32[1,256,128]{2,1,0:T(8,128)S(1)}) %tuple.82, (s32[]{:T(128)}, s32[]{:T(128)}, s32[]{:T(128)}, ...), branch_computations={%region_5.5_spmd, %region_6.8_spmd} | conditional | flops 340332288 | bytes 14553182 | solution.py:252
  153.1 4.3 %conditional.3 = ((f32[1,256]{1,0:T(1,128)S(1)}, f32[1,256]{1,0:T(1,128)S(1)}, f32[1,256,128]{2,1,0:T(8,128)S(1)})) conditional(s32[]{:T(128)} %convert_element_type.205, (f32[1,256]{1,0:T(1,128)S(1)}, f32[1,256]{1,0:T(1,128)S(1)}, f32[1,256,128]{2,1,0:T(8,128)S(1)}) %tuple.82, (s32[]{:T(128)}, s32[]{:T(128)}, s32[]{:T(128)}, ...), branch_computations={%region_5.5_spmd, %region_6.8_spmd} | conditional | flops 340332288 | bytes 14553182 | solution.py:252
  157.5 4.4 %conditional.3 = ((f32[1,256]{1,0:T(1,128)S(1)}, f32[1,256]{1,0:T(1,128)S(1)}, f32[1,256,128]{2,1,0:T(8,128)S(1)})) conditional(s32[]{:T(128)} %convert_element_type.205, (f32[1,256]{1,0:T(1,128)S(1)}, f32[1,256]{1,0:T(1,128)S(1)}, f32[1,256,128]{2,1,0:T(8,128)S(1)}) %tuple.82, (s32[]{:T(128)}, s32[]{:T(128)}, s32[]{:T(128)}, ...), branch_computations={%region_5.5_spmd, %region_6.8_spmd} | conditional | flops 340332288 | bytes 14553182 | solution.py:252
  158.9 1.5 convolution_bitcast_fusion
  161.9 4.3 %conditional.3 = ((f32[1,256]{1,0:T(1,128)S(1)}, f32[1,256]{1,0:T(1,128)S(1)}, f32[1,256,128]{2,1,0:T(8,128)S(1)})) conditional(s32[]{:T(128)} %convert_element_type.205, (f32[1,256]{1,0:T(1,128)S(1)}, f32[1,256]{1,0:T(1,128)S(1)}, f32[1,256,128]{2,1,0:T(8,128)S(1)}) %tuple.82, (s32[]{:T(128)}, s32[]{:T(128)}, s32[]{:T(128)}, ...), branch_computations={%region_5.5_spmd, %region_6.8_spmd} | conditional | flops 340332288 | bytes 14553182 | solution.py:252
  167.1 4.3 %all-to-all-start.2 = ((f32[8,256,1]{1,2,0:T(1,128)}), f32[8,256,1]{1,2,0:T(1,128)S(1)}, u32[]{:S(2)}, u32[]{:S(2)}) async-start(f32[8,256,1]{1,2,0:T(1,128)} %broadcast_in_dim.72), calls=%async_computation.2 | async-start | bytes 16384 | tf_op jit(solution)/shard_map/all_to_all | solution.py:24
  171.4 4.0 %fusion.54 = f32[256,4096]{1,0:T(8,128)} fusion(bf16[128,4096]{1,0:T(8,128)(2,1)} %param.39, f32[256,128]{1,0:T(8,128)S(1)} %get-tuple-element.364, f32[128]{0:T(128)S(1)} %copy-done.7, f32[256]{0:T(256)S(1)} %add_rsqrt_fusion.2), kind=kOutput, calls=%fused_computation.81 | convolution fusion | flops 268533760 | bytes 5375488 | tf_op jit(solution)/shard_map/dot_general | solution.py:268
  176.7 3.0 %fusion.15 = bf16[256,4096]{1,0:T(8,128)(2,1)S(1)} fusion(f32[256,4096]{1,0:T(8,128)} %fusion.54, bf16[128,4096]{1,0:T(8,128)(2,1)S(1)} %copy-done.3, f32[128]{0:T(128)S(1)} %copy-done.10, f32[256]{0:T(256)S(1)} %add_rsqrt_fusion, f32[1,256,128]{2,1,0:T(8,128)S(1)} %get-tuple-element.220, f32[256]{0:T(256)S(1)} %bitcast.96), kind=kOutput, calls=%fused_computation.28 | convolution fusion | flops 270663680 | bytes 7473664 | tf_op jit(solution)/shard_map/dot_general | solution.py:269
  179.7 30.5 %all_to_all.20 = bf16[8,32,4096]{2,1,0:T(8,128)(2,1)S(1)} all-to-all(bf16[8,32,4096]{2,1,0:T(8,128)(2,1)S(1)} %bitcast.87), channel_id=1, replica_groups=mesh['sp'=32,'tp'=8] {'tp'}, dimensions={0} | all-to-all | bytes 4194304 | tf_op jit(solution)/shard_map/all_to_all | solution.py:84
  (266 shorter events, 29.5 us)
Async XLA Ops:
  6.5 44.8 %copy-start = (bf16[4096,192]{0,1:T(8,128)(2,1)S(1)}, bf16[4096,192]{0,1:T(8,128)(2,1)}, u32[]{:S(2)}) copy-start(bf16[4096,192]{0,1:T(8,128)(2,1)} %param.32) | copy-start | bytes 4718596
  6.5 33.2 %copy-start.14 = (f32[4096]{0:T(1024)S(1)}, f32[4096]{0:T(1024)}, u32[]{:S(2)}) copy-start(f32[4096]{0:T(1024)} %param.24) | copy-start | bytes 49156
  6.5 30.9 %all-gather.3.cloned.1.call-start = ((), (), s32[]{:S(2)}) async-start(), calls=%async_computation.4 | async-start | bytes 2359296 | tf_op jit(solution)/shard_map/all_gather | solution.py:163
  7.3 127.3 %all-gather.5.cloned.1.call-start = ((), (), s32[]{:S(2)}) async-start(), calls=%async_computation.5 | async-start | bytes 5406720 | tf_op jit(solution)/shard_map/all_gather | solution.py:73
  37.5 2.3 %copy-start.1 = (bf16[256,4096]{1,0:T(8,128)(2,1)S(1)}, bf16[256,4096]{1,0:T(8,128)(2,1)}, u32[]{:S(2)}) copy-start(bf16[256,4096]{1,0:T(8,128)(2,1)} %all-gather.3.cloned.1.call-done) | copy-start | bytes 6291460
  39.7 3.6 %copy-start.11 = (bf16[4096,64]{0,1:T(8,128)(2,1)S(1)}, bf16[4096,64]{0,1:T(8,128)(2,1)}, u32[]{:S(2)}) copy-start(bf16[4096,64]{0,1:T(8,128)(2,1)} %param.34) | copy-start | bytes 1572868
  43.3 1.1 copy-start.4
  43.3 1.1 copy-start.6
  43.4 2.1 copy-start.15
  43.4 2.1 copy-start.9
  43.4 2.1 copy-start.8
  45.5 5.9 %copy-start.2 = (bf16[256,4096]{1,0:T(8,128)(2,1)S(1)}, bf16[256,4096]{1,0:T(8,128)(2,1)}, u32[]{:S(2)}) copy-start(bf16[256,4096]{1,0:T(8,128)(2,1)} %all-gather.3.cloned.1.call-done) | copy-start | bytes 6291460
  48.3 5.5 %copy-start.12 = (bf16[1,128,128]{2,1,0:T(8,128)(2,1)S(1)}, bf16[1,128,128]{2,1,0:T(8,128)(2,1)}, u32[]{:S(2)}) copy-start(bf16[1,128,128]{2,1,0:T(8,128)(2,1)} %param.29) | copy-start | bytes 98308
  48.3 5.7 %copy-start.13 = (bf16[1,128,128]{2,1,0:T(8,128)(2,1)S(1)}, bf16[1,128,128]{2,1,0:T(8,128)(2,1)}, u32[]{:S(2)}) copy-start(bf16[1,128,128]{2,1,0:T(8,128)(2,1)} %param.30) | copy-start | bytes 98308
  48.3 5.5 %collective-permute-start = (bf16[3,128]{1,0:T(4,128)(2,1)S(1)}, bf16[3,128]{1,0:T(4,128)(2,1)S(1)}, u32[]{:S(2)}, u32[]{:S(2)}) collective-permute-start(bf16[3,128]{1,0:T(4,128)(2,1)S(1)} %slice.463), channel_id=1, source_target_pairs={{0,8},{8,16},{16,24},{24,32},{32,40},{40,48},{48,56},{56,64},{64,7... | collective-permute-start | bytes 2312 | tf_op jit(solution)/shard_map/ppermute | solution.py:19
  56.8 16.1 %all-to-all-start = ((f32[32,2,128]{2,1,0:T(2,128)}), f32[32,2,128]{2,1,0:T(2,128)S(1)}, u32[]{:S(2)}, u32[]{:S(2)}) async-start(f32[32,2,128]{2,1,0:T(2,128)} %broadcast_in_dim.42), calls=%async_computation | async-start | bytes 65536 | tf_op jit(solution)/shard_map/all_to_all | solution.py:24
  76.6 8.7 %all-to-all-start.1 = ((f32[8,256,1]{1,2,0:T(1,128)}), f32[8,256,1]{1,2,0:T(1,128)S(1)}, u32[]{:S(2)}, u32[]{:S(2)}) async-start(f32[8,256,1]{1,2,0:T(1,128)} %broadcast_in_dim.45), calls=%async_computation.1 | async-start | bytes 16384 | tf_op jit(solution)/shard_map/all_to_all | solution.py:24
  145.7 1.2 slice-start
  148.7 22.7 %copy-start.7 = (f32[128]{0:T(128)S(1)}, f32[128]{0:T(128)}, u32[]{:S(2)}) copy-start(f32[128]{0:T(128)} %param.37) | copy-start | bytes 1540
  167.1 9.6 %all-to-all-start.2 = ((f32[8,256,1]{1,2,0:T(1,128)}), f32[8,256,1]{1,2,0:T(1,128)S(1)}, u32[]{:S(2)}, u32[]{:S(2)}) async-start(f32[8,256,1]{1,2,0:T(1,128)} %broadcast_in_dim.72), calls=%async_computation.2 | async-start | bytes 16384 | tf_op jit(solution)/shard_map/all_to_all | solution.py:24
  171.4 5.3 %copy-start.3 = (bf16[128,4096]{1,0:T(8,128)(2,1)S(1)}, bf16[128,4096]{1,0:T(8,128)(2,1)}, u32[]{:S(2)}) copy-start(bf16[128,4096]{1,0:T(8,128)(2,1)} %param.40) | copy-start | bytes 3145732
  171.4 5.3 %copy-start.10 = (f32[128]{0:T(128)S(1)}, f32[128]{0:T(128)}, u32[]{:S(2)}) copy-start(f32[128]{0:T(128)} %param.38) | copy-start | bytes 1540
  210.2 0.7 copy-start.5
Sparse Core Ops, SparseCore 0:
  9.2 28.2 all-gather.2
  45.6 88.9 all-gather.4
where the time goes:
time: 220 us; the launch traced here: 219 us
  waiting for transfers between devices  93.3 us (42%)
  blocking collectives  30.5 us (14%)
  matrix products  28.8 us (13%)
  local copies, waits for them, and re-layouts  22.8 us (10%)
  starting transfers between devices  21.3 us (10%)
  between operations  14.5 us (7%)
  other arithmetic  6.97 us (3%)
    all_gather x1, waiting for transfers between devices, in_one_piece(): out = lax.all_gather(both, axis, axis=dim, tiled=True)  49.2 us
    all_to_all x1, blocking collectives, sum_at_owner(): lax.all_to_all(in_blocks(shard, dim, count), axis, 0, 0, tiled=True)  30.5 us
    all_gather x1, waiting for transfers between devices, shards(): lax.all_gather(tokens, 'tp', axis=1, tiled=True).astype(jnp.float32)  30.1 us
    all_to_all x3, starting transfers between devices, from_everyone(): return lax.all_to_all(copies, axis, split_axis=0, concat_axis=0, tiled=True)  18.2 us
    all_to_all x3, waiting for transfers between devices, from_everyone(): return lax.all_to_all(copies, axis, split_axis=0, concat_axis=0, tiled=True)  11.9 us
    dot_general x5, matrix products, accumulate(): return jnp.dot(source, weight, preferred_element_type=jnp.float32)  10.7 us
    unnamed x35, local copies, waits for them, and re-layouts  8.57 us
    split x3, local copies, waits for them, and re-layouts, in_one_piece(): jnp.split(out, [sum(widths[:k]) for k in range(1, len(widths))], axis=along)  5.93 us
  transfers between devices with their start and end apart: 6, of which 6 were waited for; matrix products, arithmetic and copies ran while one was open for 6% of the time, Pallas kernels for 0%

commit v1 on v0

--- a/solution.py
+++ b/solution.py
@@ -11,6 +11,27 @@
 RATE_C = 8.0
 THETA = 10000.0
 span_limit = 2048
+
+
+def collect(array, axis, dim):
+    size, place, rows = (lax.axis_size(axis), lax.axis_index(axis), array.shape[dim])
+    forward = [(i, (i + 1) % size) for i in range(size)]
+    backward = [(i, (i - 1) % size) for i in range(size)]
+    out = jnp.zeros((*array.shape[:dim], size * rows, *array.shape[dim + 1 :]), array.dtype)
+    out = lax.dynamic_update_slice_in_dim(out, array, place * rows, axis=dim)
+    from_left = from_right = array
+    half = size // 2
+    for turn in range(1, half + 1):
+        from_left = lax.ppermute(from_left, axis, forward)
+        out = lax.dynamic_update_slice_in_dim(
+            out, from_left, (place - turn) % size * rows, axis=dim
+        )
+        if turn < size - half:
+            from_right = lax.ppermute(from_right, axis, backward)
+            out = lax.dynamic_update_slice_in_dim(
+                out, from_right, (place + turn) % size * rows, axis=dim
+            )
+    return out
 
 
 def passed_along(block, axis, distance):
@@ -160,7 +181,7 @@
     first_place = lax.axis_index("sp") * row_count
     places = first_place + jnp.arange(row_count)
     last_place = first_place + row_count - 1
-    piece_wide = lax.all_gather(tokens, "tp", axis=1, tiled=True).astype(jnp.float32)
+    piece_wide = collect(tokens, "tp", 1).astype(jnp.float32)
     piece_low = (piece_wide * pre_gain).astype(jnp.bfloat16)
 
     def accumulate(source, weight):

time: 220 us -> 216 us (0.982)
  waiting for transfers between devices: 93.3 us -> 72.2 us
  starting transfers between devices: 21.3 us -> 28.9 us
  local copies, waits for them, and re-layouts: 22.8 us -> 30.3 us
  matrix products: 28.8 us -> 31.2 us
    all_gather x1 -> x0, waiting for transfers between devices: 30.1 us -> none  [shards(): lax.all_gather(tokens, 'tp', axis=1, tiled=True).astype(jnp.float32)]
    ppermute x0 -> x7, waiting for transfers between devices: none -> 12.4 us  [the longest x4 11.1 us: collect(): from_left = lax.ppermute(from_left, axis, forward)]
    ppermute x0 -> x7, starting transfers between devices: none -> 9.01 us  [the longest x3 9 us: collect(): from_right = lax.ppermute(from_right, axis, backward)]
    dynamic_update_slice x0 -> x8, local copies, waits for them, and re-layouts: none -> 5.98 us  [the longest x4 3.01 us: collect(): lax.dynamic_update_slice_in_dim(out, from_left, (place - turn) % size * r...]
    dot_general x5, matrix products: 10.7 us -> 13.1 us  [accumulate(): return jnp.dot(source, weight, preferred_element_type=jnp.float32)]
  transfers between devices with their start and end apart: 6 -> 12, of which waited for: 6 -> 10; matrix products, arithmetic and copies ran while one was open for 6% -> 10% of each run, Pallas kernels for 0% -> 0%
where the time goes in v1:
time: 216 us; the launch traced here: 215 us
  waiting for transfers between devices  72.2 us (33%)
  matrix products  31.2 us (14%)
  blocking collectives  30.5 us (14%)
  local copies, waits for them, and re-layouts  30.3 us (14%)
  starting transfers between devices  28.9 us (13%)
  between operations  14.4 us (7%)
  other arithmetic  6.98 us (3%)
    all_gather x1, waiting for transfers between devices, in_one_piece(): out = lax.all_gather(both, axis, axis=dim, tiled=True)  48.2 us
    all_to_all x1, blocking collectives, sum_at_owner(): lax.all_to_all(in_blocks(shard, dim, count), axis, 0, 0, tiled=True)  30.5 us
    all_to_all x3, starting transfers between devices, from_everyone(): return lax.all_to_all(copies, axis, split_axis=0, concat_axis=0, tiled=True)  16.8 us
    dot_general x5, matrix products, accumulate(): return jnp.dot(source, weight, preferred_element_type=jnp.float32)  13.1 us
    all_to_all x3, waiting for transfers between devices, from_everyone(): return lax.all_to_all(copies, axis, split_axis=0, concat_axis=0, tiled=True)  11.6 us
    ppermute x4, waiting for transfers between devices, collect(): from_left = lax.ppermute(from_left, axis, forward)  11.1 us
    ppermute x3, starting transfers between devices, collect(): from_right = lax.ppermute(from_right, axis, backward)  9 us
    unnamed x35, local copies, waits for them, and re-layouts  8.59 us
  transfers between devices with their start and end apart: 12, of which 10 were waited for; matrix products, arithmetic and copies ran while one was open for 10% of the time, Pallas kernels for 0%

profile of v1, /device:TPU:228, one launch (start us, length us, event | category | flops | bytes accessed | tf_op | source)
XLA Modules:
  0.0 215.0 jit_solution(17320278730199273256)
XLA Ops:
  6.6 2.9 %collective-permute-start.1 = (bf16[256,512]{1,0:T(8,128)(2,1)}, bf16[256,512]{1,0:T(8,128)(2,1)S(1)}, u32[]{:S(2)}, u32[]{:S(2)}) collective-permute-start(bf16[256,512]{1,0:T(8,128)(2,1)} %param.23), channel_id=1, source_target_pairs={{0,7},{1,0},{2,1},{3,2},{4,3},{5,4},{6,5},{7,6},{8,15},{9,8},{10,9... | collective-permute-start | bytes 786440 | tf_op jit(solution)/shard_map/ppermute | solution.py:30
  9.5 4.3 %collective-permute-done = bf16[256,512]{1,0:T(8,128)(2,1)S(1)} collective-permute-done((bf16[256,512]{1,0:T(8,128)(2,1)}, bf16[256,512]{1,0:T(8,128)(2,1)S(1)}, u32[]{:S(2)}, u32[]{:S(2)}) %collective-permute-start) | collective-permute-done | bytes 262176 | tf_op jit(solution)/shard_map/ppermute | solution.py:25
  16.1 2.9 %collective-permute-start.3 = (bf16[256,512]{1,0:T(8,128)(2,1)S(1)}, bf16[256,512]{1,0:T(8,128)(2,1)S(1)}, u32[]{:S(2)}, u32[]{:S(2)}) collective-permute-start(bf16[256,512]{1,0:T(8,128)(2,1)S(1)} %collective-permute-done.1), channel_id=1, source_target_pairs={{0,7},{1,0},{2,1},{3,2},{4,3},{5,4},{6,5},{7,6},{8,15},{9,8},{10,9... | collective-permute-start | bytes 786440 | tf_op jit(solution)/shard_map/ppermute | solution.py:30
  22.9 3.1 %collective-permute-start.5 = (bf16[256,512]{1,0:T(8,128)(2,1)S(1)}, bf16[256,512]{1,0:T(8,128)(2,1)S(1)}, u32[]{:S(2)}, u32[]{:S(2)}) collective-permute-start(bf16[256,512]{1,0:T(8,128)(2,1)S(1)} %collective-permute-done.3), channel_id=1, source_target_pairs={{0,7},{1,0},{2,1},{3,2},{4,3},{5,4},{6,5},{7,6},{8,15},{9,8},{10,9... | collective-permute-start | bytes 786440 | tf_op jit(solution)/shard_map/ppermute | solution.py:30
  30.6 4.2 %collective-permute-done.6 = bf16[256,512]{1,0:T(8,128)(2,1)S(1)} collective-permute-done((bf16[256,512]{1,0:T(8,128)(2,1)S(1)}, bf16[256,512]{1,0:T(8,128)(2,1)S(1)}, u32[]{:S(2)}, u32[]{:S(2)}) %collective-permute-start.6) | collective-permute-done | bytes 262176 | tf_op jit(solution)/shard_map/ppermute | solution.py:25
  40.2 3.1 %multiply_reduce_fusion.1 = (f32[256]{0:T(256)S(1)}, f32[256,512]{1,0:T(8,128)S(1)}) fusion(bf16[4096,512]{1,0:T(8,128)(2,1)S(1)} %copy-done.10, bf16[256,4096]{1,0:T(8,128)(2,1)} %constant_dynamic-update-slice_fusion, f32[4096]{0:T(1024)S(1)} %copy-done.14, f32[256]{0:T(256)S(1)} %add_rsqrt_fusion.3), kind=kOutput, calls=%fused_computation.55 | convolution fusion | flops 1077280512 | bytes 6834176 | tf_op jit(solution)/shard_map/dot_general | solution.py:188
  47.2 3.1 %collective-permute-start.7 = (bf16[3,128]{1,0:T(4,128)(2,1)S(1)}, bf16[3,128]{1,0:T(4,128)(2,1)S(1)}, u32[]{:S(2)}, u32[]{:S(2)}) collective-permute-start(bf16[3,128]{1,0:T(4,128)(2,1)S(1)} %slice.463), channel_id=1, source_target_pairs={{0,8},{8,16},{16,24},{24,32},{32,40},{40,48},{48,56},{56,64},{64,7... | collective-permute-start | bytes 2312 | tf_op jit(solution)/shard_map/ppermute | solution.py:40
  55.9 9.2 %all-to-all-start = ((f32[32,2,128]{2,1,0:T(2,128)}), f32[32,2,128]{2,1,0:T(2,128)S(1)}, u32[]{:S(2)}, u32[]{:S(2)}) async-start(f32[32,2,128]{2,1,0:T(2,128)} %broadcast_in_dim.45), calls=%async_computation | async-start | bytes 65536 | tf_op jit(solution)/shard_map/all_to_all | solution.py:45
  65.3 5.3 %all-to-all-done = f32[32,2,128]{2,1,0:T(2,128)S(1)} async-done(((f32[32,2,128]{2,1,0:T(2,128)}), f32[32,2,128]{2,1,0:T(2,128)S(1)}, u32[]{:S(2)}, u32[]{:S(2)}) %all-to-all-start) | async-done | bytes 32800 | tf_op jit(solution)/shard_map/all_to_all | solution.py:45
  71.0 2.7 %multiply_reduce_fusion.2 = (f32[256]{0:T(256)S(1)}, f32[256,128]{1,0:T(8,128)S(1)}) fusion(bf16[4096,128]{1,0:T(8,128)(2,1)} %param.27, bf16[256,4096]{1,0:T(8,128)(2,1)} %constant_dynamic-update-slice_fusion, f32[4096]{0:T(1024)S(1)} %copy-done.14, f32[256]{0:T(256)S(1)} %add_rsqrt_fusion.3, f32[128]{0:T(128)S(1)} %add_bitcast_fusion, ...), kind=kOutput, calls=%fused_computation.75 | convolution fusion | flops 272105216 | bytes 3820032 | tf_op jit(solution)/shard_map/dot_general | solution.py:188
  74.3 3.3 %all-to-all-start.1 = ((f32[8,256,1]{1,2,0:T(1,128)}), f32[8,256,1]{1,2,0:T(1,128)S(1)}, u32[]{:S(2)}, u32[]{:S(2)}) async-start(f32[8,256,1]{1,2,0:T(1,128)} %broadcast_in_dim.73), calls=%async_computation.1 | async-start | bytes 16384 | tf_op jit(solution)/shard_map/all_to_all | solution.py:45
  77.7 5.1 %all-to-all-done.1 = f32[8,256,1]{1,2,0:T(1,128)S(1)} async-done(((f32[8,256,1]{1,2,0:T(1,128)}), f32[8,256,1]{1,2,0:T(1,128)S(1)}, u32[]{:S(2)}, u32[]{:S(2)}) %all-to-all-start.1) | async-done | bytes 8224 | tf_op jit(solution)/shard_map/all_to_all | solution.py:45
  82.8 48.2 %all-gather.2.cloned.1.call-done = bf16[8192,320]{0,1:T(8,128)(2,1)} async-done(((bf16[256,320]{0,1:T(8,128)(2,1)}), bf16[8192,320]{0,1:T(8,128)(2,1)}) %all-gather.2.cloned.1.call-update) | async-done | bytes 5242896 | tf_op jit(solution)/shard_map/all_gather | solution.py:94
  131.0 4.7 %split.8 = bf16[8192,256]{0,1:T(8,128)(2,1)} slice(bf16[8192,320]{0,1:T(8,128)(2,1)} %all-gather.2.cloned.1.call-done), slice={[0:8192], [0:256]} | slice | bytes 8388608 | tf_op jit(solution)/shard_map/split | solution.py:95
  135.7 6.4 %copy.31 = bf16[8192,256]{1,0:T(8,128)(2,1)} copy(bf16[8192,256]{0,1:T(8,128)(2,1)} %split.8) | data formatting | bytes 8388608
  145.1 17.6 %while.18 = (s32[]{:T(128)}, f32[1,256]{1,0:T(1,128)S(1)}, f32[1,256]{1,0:T(1,128)S(1)}, f32[1,256,128]{2,1,0:T(8,128)S(1)}, s32[]{:T(128)}, /*index=5*/bf16[819...) while((s32[]{:T(128)}, f32[1,256]{1,0:T(1,128)S(1)}, ...), condition=%wide.region_9.10_spmd.clone, body=%wide.region_4.9_spmd.clone.sunk | while | flops 340332288 | bytes 14554469 | solution.py:275
  145.1 4.4 %conditional.3 = ((f32[1,256]{1,0:T(1,128)S(1)}, f32[1,256]{1,0:T(1,128)S(1)}, f32[1,256,128]{2,1,0:T(8,128)S(1)})) conditional(s32[]{:T(128)} %convert_element_type.205, (f32[1,256]{1,0:T(1,128)S(1)}, f32[1,256]{1,0:T(1,128)S(1)}, f32[1,256,128]{2,1,0:T(8,128)S(1)}) %tuple.82, (s32[]{:T(128)}, s32[]{:T(128)}, s32[]{:T(128)}, ...), branch_computations={%region_5.5_spmd, %region_6.8_spmd} | conditional | flops 340332288 | bytes 14553182 | solution.py:273
  149.5 4.3 %conditional.3 = ((f32[1,256]{1,0:T(1,128)S(1)}, f32[1,256]{1,0:T(1,128)S(1)}, f32[1,256,128]{2,1,0:T(8,128)S(1)})) conditional(s32[]{:T(128)} %convert_element_type.205, (f32[1,256]{1,0:T(1,128)S(1)}, f32[1,256]{1,0:T(1,128)S(1)}, f32[1,256,128]{2,1,0:T(8,128)S(1)}) %tuple.82, (s32[]{:T(128)}, s32[]{:T(128)}, s32[]{:T(128)}, ...), branch_computations={%region_5.5_spmd, %region_6.8_spmd} | conditional | flops 340332288 | bytes 14553182 | solution.py:273
  153.9 4.4 %conditional.3 = ((f32[1,256]{1,0:T(1,128)S(1)}, f32[1,256]{1,0:T(1,128)S(1)}, f32[1,256,128]{2,1,0:T(8,128)S(1)})) conditional(s32[]{:T(128)} %convert_element_type.205, (f32[1,256]{1,0:T(1,128)S(1)}, f32[1,256]{1,0:T(1,128)S(1)}, f32[1,256,128]{2,1,0:T(8,128)S(1)}) %tuple.82, (s32[]{:T(128)}, s32[]{:T(128)}, s32[]{:T(128)}, ...), branch_computations={%region_5.5_spmd, %region_6.8_spmd} | conditional | flops 340332288 | bytes 14553182 | solution.py:273
  158.3 4.3 %conditional.3 = ((f32[1,256]{1,0:T(1,128)S(1)}, f32[1,256]{1,0:T(1,128)S(1)}, f32[1,256,128]{2,1,0:T(8,128)S(1)})) conditional(s32[]{:T(128)} %convert_element_type.205, (f32[1,256]{1,0:T(1,128)S(1)}, f32[1,256]{1,0:T(1,128)S(1)}, f32[1,256,128]{2,1,0:T(8,128)S(1)}) %tuple.82, (s32[]{:T(128)}, s32[]{:T(128)}, s32[]{:T(128)}, ...), branch_computations={%region_5.5_spmd, %region_6.8_spmd} | conditional | flops 340332288 | bytes 14553182 | solution.py:273
  163.5 4.3 %all-to-all-start.2 = ((f32[8,256,1]{1,2,0:T(1,128)}), f32[8,256,1]{1,2,0:T(1,128)S(1)}, u32[]{:S(2)}, u32[]{:S(2)}) async-start(f32[8,256,1]{1,2,0:T(1,128)} %broadcast_in_dim.76), calls=%async_computation.2 | async-start | bytes 16384 | tf_op jit(solution)/shard_map/all_to_all | solution.py:45
  167.8 4.0 %fusion.54 = f32[256,4096]{1,0:T(8,128)} fusion(bf16[128,4096]{1,0:T(8,128)(2,1)} %param.39, f32[256,128]{1,0:T(8,128)S(1)} %get-tuple-element.364, f32[128]{0:T(128)S(1)} %copy-done.6, f32[256]{0:T(256)S(1)} %add_rsqrt_fusion.2), kind=kOutput, calls=%fused_computation.81 | convolution fusion | flops 268533760 | bytes 5375488 | tf_op jit(solution)/shard_map/dot_general | solution.py:289
  173.1 3.0 %fusion.15 = bf16[256,4096]{1,0:T(8,128)(2,1)S(1)} fusion(f32[256,4096]{1,0:T(8,128)} %fusion.54, bf16[128,4096]{1,0:T(8,128)(2,1)S(1)} %copy-done.1, f32[128]{0:T(128)S(1)} %copy-done.9, f32[256]{0:T(256)S(1)} %add_rsqrt_fusion, f32[1,256,128]{2,1,0:T(8,128)S(1)} %get-tuple-element.220, f32[256]{0:T(256)S(1)} %bitcast.96), kind=kOutput, calls=%fused_computation.28 | convolution fusion | flops 270663680 | bytes 7473664 | tf_op jit(solution)/shard_map/dot_general | solution.py:290
  176.1 30.5 %all_to_all.20 = bf16[8,32,4096]{2,1,0:T(8,128)(2,1)S(1)} all-to-all(bf16[8,32,4096]{2,1,0:T(8,128)(2,1)S(1)} %bitcast.87), channel_id=1, replica_groups=mesh['sp'=32,'tp'=8] {'tp'}, dimensions={0} | all-to-all | bytes 4194304 | tf_op jit(solution)/shard_map/all_to_all | solution.py:105
  (286 shorter events, 50.0 us)
Async XLA Ops:
  6.5 43.8 %copy-start = (bf16[4096,192]{0,1:T(8,128)(2,1)S(1)}, bf16[4096,192]{0,1:T(8,128)(2,1)}, u32[]{:S(2)}) copy-start(bf16[4096,192]{0,1:T(8,128)(2,1)} %param.32) | copy-start | bytes 4718596
  6.5 8.8 %copy-start.2 = (bf16[256,512]{1,0:T(8,128)(2,1)S(1)}, bf16[256,512]{1,0:T(8,128)(2,1)}, u32[]{:S(2)}) copy-start(bf16[256,512]{1,0:T(8,128)(2,1)} %param.23) | copy-start | bytes 786436
  6.5 124.5 %all-gather.2.cloned.1.call-start = ((), (), s32[]{:S(2)}) async-start(), calls=%async_computation.4 | async-start | bytes 5406720 | tf_op jit(solution)/shard_map/all_gather | solution.py:94
  6.5 7.2 %collective-permute-start = (bf16[256,512]{1,0:T(8,128)(2,1)}, bf16[256,512]{1,0:T(8,128)(2,1)S(1)}, u32[]{:S(2)}, u32[]{:S(2)}) collective-permute-start(bf16[256,512]{1,0:T(8,128)(2,1)} %param.23), channel_id=1, source_target_pairs={{0,1},{1,2},{2,3},{3,4},{4,5},{5,6},{6,7},{7,0},{8,9},{9,10},{10,1... | collective-permute-start | bytes 786440 | tf_op jit(solution)/shard_map/ppermute | solution.py:25
  6.6 9.5 %collective-permute-start.1 = (bf16[256,512]{1,0:T(8,128)(2,1)}, bf16[256,512]{1,0:T(8,128)(2,1)S(1)}, u32[]{:S(2)}, u32[]{:S(2)}) collective-permute-start(bf16[256,512]{1,0:T(8,128)(2,1)} %param.23), channel_id=1, source_target_pairs={{0,7},{1,0},{2,1},{3,2},{4,3},{5,4},{6,5},{7,6},{8,15},{9,8},{10,9... | collective-permute-start | bytes 786440 | tf_op jit(solution)/shard_map/ppermute | solution.py:30
  13.8 7.0 %collective-permute-start.2 = (bf16[256,512]{1,0:T(8,128)(2,1)S(1)}, bf16[256,512]{1,0:T(8,128)(2,1)S(1)}, u32[]{:S(2)}, u32[]{:S(2)}) collective-permute-start(bf16[256,512]{1,0:T(8,128)(2,1)S(1)} %collective-permute-done), channel_id=1, source_target_pairs={{0,1},{1,2},{2,3},{3,4},{4,5},{5,6},{6,7},{7,0},{8,9},{9,10},{10,1... | collective-permute-start | bytes 786440 | tf_op jit(solution)/shard_map/ppermute | solution.py:25
  16.1 6.8 %collective-permute-start.3 = (bf16[256,512]{1,0:T(8,128)(2,1)S(1)}, bf16[256,512]{1,0:T(8,128)(2,1)S(1)}, u32[]{:S(2)}, u32[]{:S(2)}) collective-permute-start(bf16[256,512]{1,0:T(8,128)(2,1)S(1)} %collective-permute-done.1), channel_id=1, source_target_pairs={{0,7},{1,0},{2,1},{3,2},{4,3},{5,4},{6,5},{7,6},{8,15},{9,8},{10,9... | collective-permute-start | bytes 786440 | tf_op jit(solution)/shard_map/ppermute | solution.py:30
  20.8 7.0 %collective-permute-start.4 = (bf16[256,512]{1,0:T(8,128)(2,1)S(1)}, bf16[256,512]{1,0:T(8,128)(2,1)S(1)}, u32[]{:S(2)}, u32[]{:S(2)}) collective-permute-start(bf16[256,512]{1,0:T(8,128)(2,1)S(1)} %collective-permute-done.2), channel_id=1, source_target_pairs={{0,1},{1,2},{2,3},{3,4},{4,5},{5,6},{6,7},{7,0},{8,9},{9,10},{10,1... | collective-permute-start | bytes 786440 | tf_op jit(solution)/shard_map/ppermute | solution.py:25
  22.9 7.0 %collective-permute-start.5 = (bf16[256,512]{1,0:T(8,128)(2,1)S(1)}, bf16[256,512]{1,0:T(8,128)(2,1)S(1)}, u32[]{:S(2)}, u32[]{:S(2)}) collective-permute-start(bf16[256,512]{1,0:T(8,128)(2,1)S(1)} %collective-permute-done.3), channel_id=1, source_target_pairs={{0,7},{1,0},{2,1},{3,2},{4,3},{5,4},{6,5},{7,6},{8,15},{9,8},{10,9... | collective-permute-start | bytes 786440 | tf_op jit(solution)/shard_map/ppermute | solution.py:30
  26.8 11.0 %copy-start.11 = (bf16[4096,64]{0,1:T(8,128)(2,1)S(1)}, bf16[4096,64]{0,1:T(8,128)(2,1)}, u32[]{:S(2)}) copy-start(bf16[4096,64]{0,1:T(8,128)(2,1)} %param.34) | copy-start | bytes 1572868
  26.8 11.0 %copy-start.14 = (f32[4096]{0:T(1024)S(1)}, f32[4096]{0:T(1024)}, u32[]{:S(2)}) copy-start(f32[4096]{0:T(1024)} %param.24) | copy-start | bytes 49156
  27.8 7.0 %collective-permute-start.6 = (bf16[256,512]{1,0:T(8,128)(2,1)S(1)}, bf16[256,512]{1,0:T(8,128)(2,1)S(1)}, u32[]{:S(2)}, u32[]{:S(2)}) collective-permute-start(bf16[256,512]{1,0:T(8,128)(2,1)S(1)} %collective-permute-done.4), channel_id=1, source_target_pairs={{0,1},{1,2},{2,3},{3,4},{4,5},{5,6},{6,7},{7,0},{8,9},{9,10},{10,1... | collective-permute-start | bytes 786440 | tf_op jit(solution)/shard_map/ppermute | solution.py:25
  35.5 4.6 %copy-start.10 = (bf16[4096,512]{1,0:T(8,128)(2,1)S(1)}, bf16[4096,512]{1,0:T(8,128)(2,1)}, u32[]{:S(2)}) copy-start(bf16[4096,512]{1,0:T(8,128)(2,1)} %param.33) | copy-start | bytes 12582916
  40.2 4.4 %copy-start.8 = (f32[256]{0:T(256)S(1)}, f32[256]{0:T(256)}, u32[]{:S(2)}) copy-start(f32[256]{0:T(256)} %param.25) | copy-start | bytes 3076
  40.2 4.4 %copy-start.7 = (f32[4,128]{1,0:T(4,128)S(1)}, f32[4,128]{1,0:T(4,128)}, u32[]{:S(2)}) copy-start(f32[4,128]{1,0:T(4,128)} %param.28) | copy-start | bytes 6148
  47.2 5.6 %copy-start.12 = (bf16[1,128,128]{2,1,0:T(8,128)(2,1)S(1)}, bf16[1,128,128]{2,1,0:T(8,128)(2,1)}, u32[]{:S(2)}) copy-start(bf16[1,128,128]{2,1,0:T(8,128)(2,1)} %param.29) | copy-start | bytes 98308
  47.2 5.8 %copy-start.13 = (bf16[1,128,128]{2,1,0:T(8,128)(2,1)S(1)}, bf16[1,128,128]{2,1,0:T(8,128)(2,1)}, u32[]{:S(2)}) copy-start(bf16[1,128,128]{2,1,0:T(8,128)(2,1)} %param.30) | copy-start | bytes 98308
  47.2 5.6 %collective-permute-start.7 = (bf16[3,128]{1,0:T(4,128)(2,1)S(1)}, bf16[3,128]{1,0:T(4,128)(2,1)S(1)}, u32[]{:S(2)}, u32[]{:S(2)}) collective-permute-start(bf16[3,128]{1,0:T(4,128)(2,1)S(1)} %slice.463), channel_id=1, source_target_pairs={{0,8},{8,16},{16,24},{24,32},{32,40},{40,48},{48,56},{56,64},{64,7... | collective-permute-start | bytes 2312 | tf_op jit(solution)/shard_map/ppermute | solution.py:40
  55.9 14.7 %all-to-all-start = ((f32[32,2,128]{2,1,0:T(2,128)}), f32[32,2,128]{2,1,0:T(2,128)S(1)}, u32[]{:S(2)}, u32[]{:S(2)}) async-start(f32[32,2,128]{2,1,0:T(2,128)} %broadcast_in_dim.45), calls=%async_computation | async-start | bytes 65536 | tf_op jit(solution)/shard_map/all_to_all | solution.py:45
  74.3 8.5 %all-to-all-start.1 = ((f32[8,256,1]{1,2,0:T(1,128)}), f32[8,256,1]{1,2,0:T(1,128)S(1)}, u32[]{:S(2)}, u32[]{:S(2)}) async-start(f32[8,256,1]{1,2,0:T(1,128)} %broadcast_in_dim.73), calls=%async_computation.1 | async-start | bytes 16384 | tf_op jit(solution)/shard_map/all_to_all | solution.py:45
  145.1 22.7 %copy-start.6 = (f32[128]{0:T(128)S(1)}, f32[128]{0:T(128)}, u32[]{:S(2)}) copy-start(f32[128]{0:T(128)} %param.37) | copy-start | bytes 1540
  163.5 9.6 %all-to-all-start.2 = ((f32[8,256,1]{1,2,0:T(1,128)}), f32[8,256,1]{1,2,0:T(1,128)S(1)}, u32[]{:S(2)}, u32[]{:S(2)}) async-start(f32[8,256,1]{1,2,0:T(1,128)} %broadcast_in_dim.76), calls=%async_computation.2 | async-start | bytes 16384 | tf_op jit(solution)/shard_map/all_to_all | solution.py:45
  167.8 5.3 %copy-start.1 = (bf16[128,4096]{1,0:T(8,128)(2,1)S(1)}, bf16[128,4096]{1,0:T(8,128)(2,1)}, u32[]{:S(2)}) copy-start(bf16[128,4096]{1,0:T(8,128)(2,1)} %param.40) | copy-start | bytes 3145732
  167.8 5.3 %copy-start.9 = (f32[128]{0:T(128)S(1)}, f32[128]{0:T(128)}, u32[]{:S(2)}) copy-start(f32[128]{0:T(128)} %param.38) | copy-start | bytes 1540
  (5 other events, 13.0 us)
Sparse Core Ops, SparseCore 0:
  44.7 86.2 all-gather.1
